TPU v7x, 512 devices: a whole 4x8x8 slice. The times are simulated.
512 devices in a mesh: dp: 4 (over x), kv: 64 (over z, y), tp: 2 (over core).
Axes of the slice: x: 4, y: 8, z: 8, core: 2. Of those that a mesh axis runs over, the one named last changes fastest.
Arguments:
- tokens: bfloat16 [32, 1024], P('dp', 'kv'), may hold values from -6 to 6
- norm_gain: float32 [1024], P('kv'), may hold values from 0.1 to 1.9
- w_query: bfloat16 [1024, 4, 64], P('kv', 'tp'), may hold values from -0.1875 to 0.1875
- w_key: bfloat16 [1024, 4, 64], P('kv', 'tp'), may hold values from -0.1875 to 0.1875
- w_value: bfloat16 [1024, 4, 64], P('kv', 'tp'), may hold values from -0.1875 to 0.1875
- w_gate: bfloat16 [1024, 4, 64], P('kv', 'tp'), may hold values from -0.1875 to 0.1875
- w_forget: bfloat16 [1024, 4], P('kv', 'tp'), may hold values from -0.1875 to 0.1875
- w_out: bfloat16 [4, 64, 1024], P('tp', None, 'kv'), may hold values from -0.375 to 0.375
- cache_key: bfloat16 [32, 32768, 4, 64], P('dp', 'kv', 'tp'), may hold values from -6 to 6
- cache_value: bfloat16 [32, 32768, 4, 64], P('dp', 'kv', 'tp'), may hold values from -6 to 6
- cache_logf: float32 [32, 32768, 4], P('dp', 'kv', 'tp'), may hold values from -0.60003052 to 0, as said below
- lengths: int32 [32], P('dp'), may hold values from 31744 to 32767
Outputs:
- mixed: float32 [32, 1024], P('dp', 'kv')
- new_key: bfloat16 [32, 4, 64], P('dp', 'tp')
- new_value: float32 [32, 4, 64], P('dp', 'tp')
- new_logf: float32 [32, 4], P('dp', 'tp')
Inputs may be any that keep to these rules, and one draw needn't show every extreme that they name: `lengths`: each sequence has between 31744 and 32767 cached tokens. `cache_logf`: log forget gates are at most 0; most are small (down to -1 / 32768, with a typical size that differs by head), and about six positions of each sequence and head hold drops of 0.2 to 0.6.
All inputs are finite; a program needn't handle non-finite values.
Results may differ from a plain program's by a relative error of at most 0.0095.
Values sent between devices are 32-bit elements.
A program may use at most 64 MiB of HBM per device.

v0:
```python
import jax
import jax.numpy as jnp
from jax import lax
from jax.sharding import Mesh
from jax.sharding import PartitionSpec as P

D = 1024
HEAD_DIM = 64
KV = ("kv_0", "kv_1")


eps = 1e-06
very_low = -1e30


def by_axis(value, axes):
    for axis in axes:
        value = lax.psum(value, axis)
    return value


def neutral_like(value, identity):
    return jax.tree.map(
        lambda part, zero: jnp.zeros_like(part) + jnp.asarray(zero, part.dtype), value, identity
    )


def prefix_by_axis(value, axes, combine, identity, reverse):
    before = start = neutral_like(value, identity)
    so_far = value
    for axis in reversed(axes):
        devices, here = lax.axis_size(axis), lax.axis_index(axis)
        pieces = jax.tree.map(lambda part: lax.all_gather(part, axis), so_far)
        inside, so_far = start, start
        for k in reversed(range(devices)) if reverse else range(devices):
            passed = k > here if reverse else k < here
            so_far = combine(so_far, jax.tree.map(lambda part: part[k], pieces))
            inside = jax.tree.map(lambda new, old: jnp.where(passed, new, old), so_far, inside)
        before = combine(inside, before)
    return before


def one_axis_at_a_time(value, axes):
    for axis in axes:
        value = lax.pmax(value, axis)
    return value


def total_of_pieces(value, axis):
    return lax.all_gather(value, axis).sum(0)


def add_terms(earlier, later):
    return earlier + later


def head_norm(values):
    return values * lax.rsqrt(jnp.mean(values * values, axis=-1, keepdims=True) + eps)


def on_device(
    tokens,
    norm_gain,
    w_query,
    w_key,
    w_value,
    w_gate,
    w_forget,
    w_out,
    cache_key,
    cache_value,
    cache_logf,
    lengths,
):
    wide_tokens = tokens.astype(jnp.float32)
    local_squares = jnp.sum(wide_tokens * wide_tokens, axis=1)
    total_squares = by_axis(local_squares, KV)
    inv_root = lax.rsqrt(total_squares / D + eps)
    normed = (wide_tokens * inv_root[:, None] * norm_gain).astype(jnp.bfloat16)
    part_query = jnp.einsum("sd,dhe->she", normed, w_query, preferred_element_type=jnp.float32)
    part_key = jnp.einsum("sd,dhe->she", normed, w_key, preferred_element_type=jnp.float32)
    part_value = jnp.einsum("sd,dhe->she", normed, w_value, preferred_element_type=jnp.float32)
    part_gate = jnp.einsum("sd,dhe->she", normed, w_gate, preferred_element_type=jnp.float32)
    part_forget = jnp.dot(normed, w_forget, preferred_element_type=jnp.float32)
    proj_query, proj_key, proj_value, proj_gate, proj_forget = (
        by_axis(part_query, KV),
        by_axis(part_key, KV),
        by_axis(part_value, KV),
        by_axis(part_gate, KV),
        by_axis(part_forget, KV),
    )
    query_vec = head_norm(proj_query).astype(jnp.bfloat16)
    key_new = head_norm(proj_key).astype(jnp.bfloat16)
    value_new = proj_value
    gate_silu = jax.nn.silu(proj_gate)
    logf_new = jax.nn.log_sigmoid(proj_forget)
    span = cache_key.shape[1]
    shard_index = lax.axis_index(KV)
    positions = shard_index * span + jnp.arange(span, dtype=jnp.int32)
    in_range = positions[None, :] < lengths[:, None]
    masked_logf = jnp.where(in_range[:, :, None], cache_logf, jnp.float32(0.0))
    running = jnp.cumsum(masked_logf, axis=1)
    shard_total = running[:, -1, :]
    later_outside = prefix_by_axis(shard_total, KV, add_terms, jnp.zeros_like(shard_total), True)
    forget_bias = (
        logf_new[:, None, :] + (shard_total[:, None, :] - running) + later_outside[:, None, :]
    )
    scores = jnp.einsum(
        "she,sphe->shp", query_vec, cache_key, preferred_element_type=jnp.float32
    ) * HEAD_DIM ** (-0.5)
    scores = scores + jnp.transpose(forget_bias, (0, 2, 1))
    score_new = jnp.sum(
        query_vec.astype(jnp.float32) * key_new.astype(jnp.float32), axis=-1
    ) * HEAD_DIM ** (-0.5)
    holder = lengths // span == shard_index
    range_mask = in_range[:, None, :]
    local_peak = jnp.max(jnp.where(range_mask, scores, very_low), axis=-1)
    local_peak = jnp.maximum(local_peak, jnp.where(holder[:, None], score_new, very_low))

    def partial_terms(peak):
        weights = jnp.where(range_mask, jnp.exp(scores - peak[..., None]), jnp.float32(0.0))
        weight_new = jnp.where(holder[:, None], jnp.exp(score_new - peak), jnp.float32(0.0))
        denominator = jnp.sum(weights, axis=-1) + weight_new
        weighted = jnp.einsum(
            "shp,sphe->she",
            weights.astype(jnp.bfloat16),
            cache_value,
            preferred_element_type=jnp.float32,
        )
        weighted = weighted + weight_new[..., None] * value_new
        return (denominator, weighted)

    peak = one_axis_at_a_time(local_peak, KV)
    local_den, local_sum = partial_terms(peak)
    denominator, weighted = (by_axis(local_den, KV), by_axis(local_sum, KV))
    attended = weighted / denominator[..., None]
    gated = (head_norm(attended) * gate_silu).astype(jnp.bfloat16)
    partial_out = jnp.einsum("she,hed->sd", gated, w_out, preferred_element_type=jnp.float32)
    mixed = total_of_pieces(partial_out, "tp")
    return (mixed, key_new, value_new, logf_new)


def solution(mesh):
    finer = Mesh(
        mesh.devices.reshape(mesh.shape["dp"], 8, 8, mesh.shape["tp"]), ("dp", "kv_0", "kv_1", "tp")
    )
    return jax.shard_map(
        on_device,
        mesh=finer,
        in_specs=(
            P("dp", KV),
            P(KV),
            P(KV, "tp", None),
            P(KV, "tp", None),
            P(KV, "tp", None),
            P(KV, "tp", None),
            P(KV, "tp"),
            P("tp", None, KV),
            P("dp", KV, "tp", None),
            P("dp", KV, "tp", None),
            P("dp", KV, "tp"),
            P("dp"),
        ),
        out_specs=(P("dp", KV), P("dp", "tp", None), P("dp", "tp", None), P("dp", "tp")),
        check_vma=False,
    )
```

profile of v0, /device:TPU:1, one launch (start us, length us, event | category | flops | bytes accessed | tf_op | source)
XLA Modules:
  0.0 236.8 jit_solution(5692271520904168080)
XLA Ops:
  0.6 0.0 copy-start
  0.6 0.0 copy-start.2
  0.7 0.9 fusion.19
  1.5 20.2 %psum.112 = f32[8]{0:T(128)S(1)} all-reduce(f32[8]{0:T(128)S(1)} %fusion.19), channel_id=1, replica_groups=mesh['dp'=4,'kv_0'=8,'kv_1'=8,'tp'=2] {'kv_0'}, use_global_device_ids=true, to_apply=%region_1.0 | all-reduce | flops 8 | bytes 64 | tf_op jit(solution)/shard_map/psum | solution.py:18
  21.8 13.8 %psum.113 = f32[8]{0:T(128)S(1)} all-reduce(f32[8]{0:T(128)S(1)} %psum.112), channel_id=1, replica_groups=mesh['dp'=4,'kv_0'=8,'kv_1'=8,'tp'=2] {'kv_1'}, use_global_device_ids=true, to_apply=%region_2.0 | all-reduce | flops 8 | bytes 64 | tf_op jit(solution)/shard_map/psum | solution.py:18
  35.6 0.8 fusion.21
  36.4 0.0 copy-done.2
  36.4 0.1 fusion.11
  36.5 0.7 copy-done.7
  37.2 0.1 broadcast_compare_fusion
  37.4 2.3 reduce-window.6
  39.6 0.1 slice.84
  39.7 0.1 copy.48
  39.9 0.1 bitcast_bitcast_fusion
  39.9 0.2 slice_reduce_fusion
  40.1 18.1 %all-gather = f32[64,1,2]{1,0,2:T(8,128)S(1)} all-gather(f32[8,1,2]{1,0,2:T(8,128)S(1)} %get-tuple-element.45), channel_id=2, replica_groups=mesh['dp'=4,'kv_0'=8,'kv_1'=8,'tp'=2] {'kv_1'}, dimensions={0}, use_global_device_ids=true | all-gather | bytes 576 | tf_op jit(solution)/shard_map/all_gather | solution.py:33
  58.2 0.1 select_reduce_fusion.1
  58.3 10.1 %all_gather.14 = f32[8,8,2]{1,2,0:T(2,128)S(1)} all-gather(f32[1,8,2]{1,2,0:T(2,128)S(1)} %bitcast.57), channel_id=1, replica_groups=mesh['dp'=4,'kv_0'=8,'kv_1'=8,'tp'=2] {'kv_0'}, dimensions={0}, use_global_device_ids=true | all-gather | bytes 576 | tf_op jit(solution)/shard_map/all_gather | solution.py:33
  68.4 0.7 copy-done.3
  69.1 0.1 fusion.17
  69.2 0.5 copy-done.10
  69.8 0.1 fusion.37
  69.9 0.1 fusion.15
  70.0 0.6 copy-done.5
  70.6 0.1 fusion.13
  70.7 21.2 %all-reduce.3 = (f32[8,2,64]{2,0,1:T(8,128)S(1)}, f32[8,2]{0,1:T(2,128)S(1)}, f32[8,2,64]{2,0,1:T(8,128)S(1)}, f32[8,2,64]{2,0,1:T(8,128)S(1)}) all-reduce(f32[8,2,64]{2,0,1:T(8,128)S(1)} %fusion.17, f32[8,2]{0,1:T(2,128)S(1)} %fusion.37, f32[8,2,64]{2,0,1:T(8,128)S(1)} %fusion.15, ...), channel_id=1, replica_groups=mesh['dp'=4,'kv_0'=8,'kv_1'=8,'tp'=2] {'kv_0'}, use_global_device_ids=true, to_apply=%region_3.0 | all-reduce | flops 3088 | bytes 24704 | tf_op jit(solution)/shard_map/psum | solution.py:18
  91.9 20.8 %all-reduce.1 = (f32[8,2,64]{2,0,1:T(8,128)S(1)}, f32[8,2]{0,1:T(2,128)S(1)}, f32[8,2,64]{2,0,1:T(8,128)S(1)}, f32[8,2,64]{2,0,1:T(8,128)S(1)}) all-reduce(f32[8,2,64]{2,0,1:T(8,128)S(1)} %get-tuple-element.32, f32[8,2]{0,1:T(2,128)S(1)} %get-tuple-element.33, ...), channel_id=1, replica_groups=mesh['dp'=4,'kv_0'=8,'kv_1'=8,'tp'=2] {'kv_1'}, use_global_device_ids=true, to_apply=%region_4.0 | all-reduce | flops 3088 | bytes 24704 | tf_op jit(solution)/shard_map/psum | solution.py:18
  112.8 0.0 copy-start.6
  112.8 0.1 multiply_reduce_fusion.2
  112.9 0.2 multiply_reduce_fusion.1
  113.0 0.0 copy-done
  113.0 0.3 fusion.9
  113.3 0.0 copy-done.6
  113.3 0.2 select_reduce_fusion
  113.5 10.7 %pmax.14 = f32[8,2]{0,1:T(2,128)S(1)} all-reduce(f32[8,2]{0,1:T(2,128)S(1)} %select_maximum_fusion), channel_id=1, replica_groups=mesh['dp'=4,'kv_0'=8,'kv_1'=8,'tp'=2] {'kv_0'}, use_global_device_ids=true, to_apply=%region_15.16 | all-reduce | flops 16 | bytes 128 | tf_op jit(solution)/shard_map/pmax | solution.py:45
  124.2 10.7 %pmax.15 = f32[8,2]{0,1:T(2,128)S(1)} all-reduce(f32[8,2]{0,1:T(2,128)S(1)} %pmax.14), channel_id=1, replica_groups=mesh['dp'=4,'kv_0'=8,'kv_1'=8,'tp'=2] {'kv_1'}, use_global_device_ids=true, to_apply=%region_16.17 | all-reduce | flops 16 | bytes 128 | tf_op jit(solution)/shard_map/pmax | solution.py:45
  134.9 0.2 fusion.5
  135.0 0.4 fusion.3
  135.4 0.1 bitcast_add_fusion
  135.5 22.0 %all-reduce.2 = (f32[8,2,64]{2,0,1:T(8,128)S(1)}, f32[8,2,64]{2,0,1:T(8,128)S(1)}, f32[8,2]{0,1:T(2,128)S(1)}) all-reduce(f32[8,2,64]{2,0,1:T(8,128)S(1)} %fusion.11, f32[8,2,64]{2,0,1:T(8,128)S(1)} %bitcast_add_fusion, f32[8,2]{0,1:T(2,128)S(1)} %get-tuple-element.36), channel_id=1, replica_groups=mesh['dp'=4,'kv_0'=8,'kv_1'=8,'tp'=2] {'kv_0'}, use_global_device_ids=true, to_apply=%region_25.26 | all-reduce | flops 2064 | bytes 16512 | tf_op jit(solution)/shard_map/psum | solution.py:18
  157.5 21.8 %all-reduce = (f32[8,2,64]{2,0,1:T(8,128)S(1)}, f32[8,2,64]{2,0,1:T(8,128)S(1)}, f32[8,2]{0,1:T(2,128)S(1)}) all-reduce(f32[8,2,64]{2,0,1:T(8,128)S(1)} %get-tuple-element.29, f32[8,2,64]{2,0,1:T(8,128)S(1)} %get-tuple-element.30, f32[8,2]{0,1:T(2,128)S(1)} %get-tuple-element.31), channel_id=1, replica_groups=mesh['dp'=4,'kv_0'=8,'kv_1'=8,'tp'=2] {'kv_1'}, use_global_device_ids=true, to_apply=%region_26.27 | all-reduce | flops 2064 | bytes 16512 | tf_op jit(solution)/shard_map/psum | solution.py:18
  179.3 0.2 multiply_reduce_fusion
  179.5 0.5 copy-done.9
  180.0 0.2 convolution_bitcast_fusion
  180.2 54.9 %all-gather.1 = f32[16,16]{1,0:T(8,128)S(1)} all-gather(f32[8,16]{1,0:T(8,128)S(1)} %convolution_bitcast_fusion), channel_id=3, replica_groups=mesh['dp'=4,'kv_0'=8,'kv_1'=8,'tp'=2] {'tp'}, dimensions={0}, use_global_device_ids=true | all-gather | bytes 1536 | tf_op jit(solution)/shard_map/all_gather | solution.py:50
  235.0 0.6 bitcast_reduce_fusion
  235.6 0.6 copy.54
  236.2 0.6 copy.55
  (27 shorter events, 0.2 us)
Async XLA Ops:
  0.6 112.4 %copy-start = (bf16[8,512,2,64]{1,3,2,0:T(8,128)(2,1)S(1)}, bf16[8,512,2,64]{1,3,2,0:T(8,128)(2,1)}, u32[]{:S(2)}) copy-start(bf16[8,512,2,64]{1,3,2,0:T(8,128)(2,1)} %param.20) | copy-start | bytes 3145732
  0.6 35.8 %copy-start.2 = (bf16[16,2,64]{2,1,0:T(2,128)(2,1)S(1)}, bf16[16,2,64]{2,1,0:T(2,128)(2,1)}, u32[]{:S(2)}) copy-start(bf16[16,2,64]{2,1,0:T(2,128)(2,1)} %param.17) | copy-start | bytes 12292
  0.7 36.6 %copy-start.1 = (f32[8,512,2]{1,2,0:T(2,128)S(1)}, f32[8,512,2]{1,2,0:T(2,128)}, u32[]{:S(2)}) copy-start(f32[8,512,2]{1,2,0:T(2,128)} %param.22) | copy-start | bytes 98308
  36.5 0.7 copy-start.7
  68.4 0.7 copy-start.3
  69.1 0.7 copy-start.10
  69.1 0.8 copy-start.4
  69.9 0.7 copy-start.5
  69.9 65.1 %copy-start.8 = (bf16[8,512,2,64]{1,3,2,0:T(8,128)(2,1)S(1)}, bf16[8,512,2,64]{1,3,2,0:T(8,128)(2,1)}, u32[]{:S(2)}) copy-start(bf16[8,512,2,64]{1,3,2,0:T(8,128)(2,1)} %param.21) | copy-start | bytes 3145732
  112.8 0.6 copy-start.6
  179.3 0.7 copy-start.9
where the time goes:
time: 237 us
  blocking collectives  224 us (95%)
  other arithmetic  5.72 us (2%)
  local copies, waits for them, and re-layouts  4.66 us (2%)
    psum x6, blocking collectives, by_axis(): value = lax.psum(value, axis)  120 us
    all_gather x1, blocking collectives, total_of_pieces(): return lax.all_gather(value, axis).sum(0)  54.9 us
    all_gather x2, blocking collectives, prefix_by_axis(): pieces = jax.tree.map(lambda part: lax.all_gather(part, axis), so_far)  28.2 us
    pmax x2, blocking collectives, one_axis_at_a_time(): value = lax.pmax(value, axis)  21.3 us

commit v1 on v0

v1 whole, which is shorter than its diff:
```python
import jax
import jax.numpy as jnp
from jax import lax
from jax.experimental import pallas as pl
from jax.experimental.pallas import tpu as pltpu
from jax.sharding import Mesh
from jax.sharding import PartitionSpec as P

D = 1024
HD = 64
N = 8
KV = ("kv_0", "kv_1")
EPS = 1e-6
MESH = pl.DeviceIdType.MESH
FAR_FIRST = (4, 3, 5, 2, 6, 1, 7)
HI = lax.Precision.HIGHEST


def iota(shape, axis):
    return lax.broadcasted_iota(jnp.int32, shape, axis)


def lane_sum(x):
    return jnp.sum(x, axis=1, keepdims=True)


def to_row(cols):
    sub, lane = iota((8, 128), 0), iota((8, 128), 1)
    tile = jnp.zeros((8, 128), jnp.float32)
    for c, col in enumerate(cols):
        tile = jnp.where(lane == 8 * c + sub, col, tile)
    return jnp.sum(tile, axis=0, keepdims=True)


def from_row(row, c):
    sub, lane = iota((8, 128), 0), iota((8, 128), 1)
    return lane_sum(jnp.where(lane == 8 * c + sub, row, 0.0))


def by_head(first, second):
    return jnp.where(iota((8, 128), 1) < HD, first, second)


def head_mean(x):
    left = lane_sum(jnp.where(iota((8, 128), 1) < HD, x, 0.0))
    right = lane_sum(jnp.where(iota((8, 128), 1) < HD, 0.0, x))
    return by_head(left, right) * (1.0 / HD)


def kernel(
    tok_h, gain_h, wq_h, wk_h, wv_h, wg_h, wf_h, wo_h, key_h, val_h, logf_h, len_h,
    mixed_o, nkey_o, nval_o, nlogf_o,
    tok, gain, wq, wk, wv, wg, wf, wo, key, val, logf, lens, small_sem, logf_sem, key_sem, val_sem,
    crit, rs_src, rs, ar, ag, tpb, bias_s, side, send_sem, recv_sem,
):
    z, y, t = lax.axis_index("kv_0"), lax.axis_index("kv_1"), lax.axis_index("tp")
    barrier = pltpu.get_barrier_semaphore()
    for d in FAR_FIRST:
        pl.semaphore_signal(barrier, 1, device_id={"kv_1": lax.rem(y + d, N)}, device_id_type=MESH)
        pl.semaphore_signal(barrier, 1, device_id={"kv_0": lax.rem(z + d, N)}, device_id_type=MESH)
    pl.semaphore_signal(barrier, 1, device_id={"tp": 1 - t}, device_id_type=MESH)

    smalls = [
        pltpu.make_async_copy(a, b, small_sem.at[i])
        for i, (a, b) in enumerate(
            [(tok_h, tok), (gain_h, gain), (wq_h, wq), (wk_h, wk), (wv_h, wv), (wg_h, wg), (wf_h, wf),
             (len_h, lens), (wo_h, wo)]
        )
    ]
    for copy in smalls:
        copy.start()
    logf_copy = pltpu.make_async_copy(logf_h, logf, logf_sem)
    logf_copy.start()
    key_copies = [
        pltpu.make_async_copy(key_h.at[pl.ds(i * 256, 256)], key.at[pl.ds(i * 256, 256)], key_sem.at[i])
        for i in range(4)
    ]
    val_copies = [
        pltpu.make_async_copy(val_h.at[pl.ds(i * 256, 256)], val.at[pl.ds(i * 256, 256)], val_sem.at[i])
        for i in range(4)
    ]
    for copy in key_copies + val_copies:
        copy.start()

    def exchange(stage, buf, src, axis, me):
        for d in FAR_FIRST:
            pltpu.make_async_remote_copy(
                src, buf.at[me], send_sem.at[stage], recv_sem.at[stage],
                device_id={axis: lax.rem(me + d, N)}, device_id_type=MESH,
            ).start()

    def arrived(stage, buf):
        seven = buf.at[pl.ds(0, N - 1)]
        pltpu.make_async_copy(seven, seven, recv_sem.at[stage]).wait()

    def sent(stage, buf):
        seven = buf.at[pl.ds(0, N - 1)]
        pltpu.make_async_copy(seven, seven, send_sem.at[stage]).wait()

    for copy in smalls:
        copy.wait()
    wide = tok[...].astype(jnp.float32)
    squares = lane_sum(wide * wide)
    scaled = wide * gain[...]
    narrow = scaled.astype(jnp.bfloat16)

    def project(w):
        w32 = w[...].astype(jnp.float32)
        halves = [
            jnp.dot(narrow, w32[:, h, :].astype(jnp.bfloat16), preferred_element_type=jnp.float32)
            for h in range(2)
        ]
        return jnp.concatenate(halves, axis=1)

    wf32 = wf[...].astype(jnp.float32)
    narrow32 = narrow.astype(jnp.float32)
    forget = [lane_sum(narrow32 * wf32[h : h + 1, :]) for h in range(2)]

    sub8, lane8 = iota((8, 8), 0), iota((8, 8), 1)
    len_col = lane_sum(jnp.where(sub8 == lane8, lens[...].astype(jnp.float32), 0.0))
    len_col = jnp.concatenate([len_col, len_col], axis=0)
    first = (z * N + y) * 512
    position = (iota((16, 512), 1) + first).astype(jnp.float32)
    valid = position < len_col
    logf_copy.wait()
    gates = jnp.concatenate([logf[:, 0, :], logf[:, 1, :]], axis=0)
    gates = jnp.where(valid, gates, 0.0)
    blocks = jnp.concatenate([gates[:, 128 * j : 128 * (j + 1)] for j in range(4)], axis=0)
    row_i, col_i = iota((128, 256), 0), iota((128, 256), 1)
    after = jnp.where((col_i >= 128) | (row_i > col_i), 1.0, 0.0).astype(jnp.float32)
    sums = jnp.dot(blocks, after, preferred_element_type=jnp.float32, precision=HI)
    later = jnp.zeros((16, 128), jnp.float32)
    for j in (3, 2, 1, 0):
        bias_s[:, 128 * j : 128 * (j + 1)] = sums[16 * j : 16 * (j + 1), :128] + later
        later = later + sums[16 * j : 16 * (j + 1), 128:]

    crit[0, y, 0:8, :] = project(wq)
    crit[0, y, 8:9, :] = to_row([squares, forget[0], forget[1], later[:8], later[8:]])
    pieces = [project(wk), project(wv), project(wg)]
    for j in range(N):
        for i, piece in enumerate(pieces):
            rs_src[j, :, 128 * i : 128 * (i + 1)] = piece[j : j + 1, :]

    pl.semaphore_wait(barrier, 15)
    exchange(0, crit.at[0], crit.at[0, y], "kv_1", y)
    for d in FAR_FIRST:
        other = lax.rem(y + d, N)
        pltpu.make_async_remote_copy(
            rs_src.at[other], rs.at[y], send_sem.at[4], recv_sem.at[4],
            device_id={"kv_1": other}, device_id_type=MESH,
        ).start()
    rs[y] = rs_src[y]

    def total(stage):
        acc = crit[stage, 0]
        for j in range(1, N):
            acc = acc + crit[stage, j]
        return acc

    def later_rows(stage, me):
        acc = jnp.zeros((1, 128), jnp.float32)
        for j in range(1, N):
            acc = acc + jnp.where(j > me, crit[stage, j, 8:9, :], 0.0)
        return acc

    arrived(0, crit.at[0])
    crit[1, z] = total(0)
    exchange(1, crit.at[1], crit.at[1, z], "kv_0", z)

    arrived(4, rs)
    row = rs[0]
    for j in range(1, N):
        row = row + rs[j]
    ar[z] = row
    exchange(5, ar, ar.at[z], "kv_0", z)

    later_y = later_rows(0, y)
    for copy in key_copies:
        copy.wait()

    arrived(1, crit.at[1])
    summed = total(1)
    info = summed[8:9, :]
    q_sum = summed[0:8, :]
    mean_square = from_row(info, 0) * (1.0 / D)
    inv_square = 1.0 / (mean_square + EPS)
    inv_root = lax.rsqrt(mean_square + EPS)
    q_mean = head_mean(q_sum * q_sum)
    query = q_sum * (inv_root * lax.rsqrt(q_mean * inv_square + EPS))
    query = query.astype(jnp.bfloat16)
    side[0] = query.astype(jnp.float32)
    new_logf = []
    for h in range(2):
        logit = from_row(info, 1 + h) * inv_root
        new_logf.append(jnp.minimum(logit, 0.0) - jnp.log1p(jnp.exp(-jnp.abs(logit))))
    later_all = later_y + later_rows(1, z)
    extra = jnp.concatenate([from_row(later_all, 3) + new_logf[0], from_row(later_all, 4) + new_logf[1]], axis=0)

    q32 = side[0]
    double = jnp.concatenate([q32, q32], axis=0)
    row16, lane16 = iota((16, 128), 0), iota((16, 128), 1)
    own_head = (row16 // 8) == (lane16 // HD)
    lhs = jnp.concatenate(
        [jnp.where(own_head & (row16 % 8 == b), double, 0.0).astype(jnp.bfloat16) for b in range(8)], axis=1
    )
    scores = jnp.dot(lhs, key[...], preferred_element_type=jnp.float32) * (HD ** -0.5)
    weights = jnp.where(valid, jnp.exp(scores + (bias_s[...] + extra)), 0.0)
    den = lane_sum(weights)
    for copy in val_copies:
        copy.wait()
    wide_out = lax.dot_general(
        weights.astype(jnp.bfloat16), val[...], (((1,), (1,)), ((), ())), preferred_element_type=jnp.float32
    )
    acc = jnp.zeros((16, 128), jnp.float32)
    for b in range(8):
        acc = jnp.where(own_head & (row16 % 8 == b), wide_out[:, 128 * b : 128 * (b + 1)], acc)
    crit[2, y, 0:8, :] = acc[:8] + acc[8:]
    crit[2, y, 8:9, :] = to_row([den[:8], den[8:]])
    exchange(2, crit.at[2], crit.at[2, y], "kv_1", y)

    arrived(5, ar)
    row = ar[0]
    for j in range(1, N):
        row = row + ar[j]
    ag[y] = row
    exchange(6, ag, ag.at[y], "kv_1", y)

    arrived(2, crit.at[2])
    crit[3, z] = total(2)
    exchange(3, crit.at[3], crit.at[3, z], "kv_0", z)

    arrived(6, ag)
    everything = jnp.concatenate([ag[j] for j in range(N)], axis=0)
    k_sum = everything[:, 0:128]
    value_new = everything[:, 128:256] * inv_root
    gate = everything[:, 256:384] * inv_root
    k_mean = head_mean(k_sum * k_sum)
    key_new = (k_sum * (inv_root * lax.rsqrt(k_mean * inv_square + EPS))).astype(jnp.bfloat16)
    key_new32 = key_new.astype(jnp.float32)
    silu = gate * jax.nn.sigmoid(gate)
    score_new = head_mean(side[0] * key_new32) * (HD ** 0.5)
    weight_new = jnp.exp(score_new)
    nkey_o[...] = key_new32
    nval_o[...] = value_new
    nlogf_o[...] = by_head(new_logf[0], new_logf[1])

    arrived(3, crit.at[3])
    summed = total(3)
    info = summed[8:9, :]
    denominator = by_head(from_row(info, 0), from_row(info, 1)) + weight_new
    attended = (summed[0:8, :] + weight_new * value_new) / denominator
    gated = attended * lax.rsqrt(head_mean(attended * attended) + EPS) * silu
    gated = gated.astype(jnp.bfloat16)
    mine = lax.dot_general(
        gated[:, :HD], wo[0], (((1,), (1,)), ((), ())), preferred_element_type=jnp.float32
    ) + lax.dot_general(
        gated[:, HD:], wo[1], (((1,), (1,)), ((), ())), preferred_element_type=jnp.float32
    )
    tpb[t] = mine
    last = pltpu.make_async_remote_copy(
        tpb.at[t], tpb.at[t], send_sem.at[7], recv_sem.at[7], device_id={"tp": 1 - t}, device_id_type=MESH
    )
    last.start()
    for stage in range(4):
        sent(stage, crit.at[stage])
    sent(4, rs)
    sent(5, ar)
    sent(6, ag)
    last.wait()
    mixed_o[...] = tpb[0] + tpb[1]


def on_device(tokens, norm_gain, w_query, w_key, w_value, w_gate, w_forget, w_out, cache_key, cache_value, cache_logf, lengths):
    span = cache_key.shape[1]
    keys = jnp.transpose(cache_key, (0, 2, 3, 1)).reshape(8 * 2 * HD, span)
    values = jnp.transpose(cache_value, (0, 2, 3, 1)).reshape(8 * 2 * HD, span)
    logf = jnp.transpose(cache_logf, (0, 2, 1))
    args = (
        tokens, norm_gain.reshape(1, -1), w_query, w_key, w_value, w_gate, w_forget.T,
        jnp.transpose(w_out, (0, 2, 1)), keys, values, logf, lengths.reshape(1, -1),
    )
    f32 = jnp.float32
    tile = jax.ShapeDtypeStruct((8, 128), f32)
    scratch = [pltpu.VMEM(a.shape, a.dtype) for a in args] + [
        pltpu.SemaphoreType.DMA((9,)),
        pltpu.SemaphoreType.DMA(()),
        pltpu.SemaphoreType.DMA((4,)),
        pltpu.SemaphoreType.DMA((4,)),
        pltpu.VMEM((4, N, 9, 128), f32),
        pltpu.VMEM((N, 1, 384), f32),
        pltpu.VMEM((N, 1, 384), f32),
        pltpu.VMEM((N, 1, 384), f32),
        pltpu.VMEM((N, 1, 384), f32),
        pltpu.VMEM((2, 8, 16), f32),
        pltpu.VMEM((16, 512), f32),
        pltpu.VMEM((1, 8, 128), f32),
        pltpu.SemaphoreType.DMA((8,)),
        pltpu.SemaphoreType.DMA((8,)),
    ]
    mixed, nkey, nval, nlogf = pl.pallas_call(
        kernel,
        out_shape=(jax.ShapeDtypeStruct((8, 16), f32), tile, tile, tile),
        in_specs=[pl.BlockSpec(memory_space=pltpu.HBM)] * 12,
        out_specs=tuple(pl.BlockSpec(memory_space=pltpu.VMEM) for _ in range(4)),
        scratch_shapes=scratch,
        compiler_params=pltpu.CompilerParams(collective_id=0, has_side_effects=True),
        name="decode_step",
    )(*args)
    key_new = nkey.reshape(8, 2, HD).astype(jnp.bfloat16)
    value_new = nval.reshape(8, 2, HD)
    return mixed, key_new, value_new, nlogf.reshape(8, 2, HD)[:, :, 0]


def solution(mesh):
    finer = Mesh(
        mesh.devices.reshape(mesh.shape["dp"], N, N, mesh.shape["tp"]), ("dp", "kv_0", "kv_1", "tp")
    )
    return jax.shard_map(
        on_device,
        mesh=finer,
        in_specs=(
            P("dp", KV), P(KV), P(KV, "tp", None), P(KV, "tp", None), P(KV, "tp", None), P(KV, "tp", None),
            P(KV, "tp"), P("tp", None, KV), P("dp", KV, "tp", None), P("dp", KV, "tp", None),
            P("dp", KV, "tp"), P("dp"),
        ),
        out_specs=(P("dp", KV), P("dp", "tp", None), P("dp", "tp", None), P("dp", "tp")),
        check_vma=False,
    )
```

time: 237 us -> 39.8 us (0.17)
  blocking collectives: 224 us -> 0 us
  Pallas kernels: 0 us -> 35.4 us
  other arithmetic: 5.72 us -> 0.01 us
    psum x6 -> x0, blocking collectives: 120 us -> none  [by_axis(): value = lax.psum(value, axis)]
    all_gather x3 -> x0, blocking collectives: 83.1 us -> none  [the longest x1 54.9 us: total_of_pieces(): return lax.all_gather(value, axis).sum(0)]
    pallas_call x0 -> x1, Pallas kernels: none -> 35.4 us  [on_device(): pl.pallas_call(kernel, out_shape=(jax.ShapeDtypeStruct((8, 16), f32), til...]
    pmax x2 -> x0, blocking collectives: 21.3 us -> none  [one_axis_at_a_time(): value = lax.pmax(value, axis)]
    unnamed x24 -> x8, local copies, waits for them, and re-layouts: 4.25 us -> 1.28 us
    another operation x3 -> x0, other arithmetic: 2.39 us -> none
where the time goes in v1:
time: 39.8 us; the launch traced here: 39.5 us
  Pallas kernels  35.4 us (89%)
  local copies, waits for them, and re-layouts  3.39 us (9%)
  between operations  0.65 us (2%)
    pallas_call x1, Pallas kernels, on_device(): pl.pallas_call(kernel, out_shape=(jax.ShapeDtypeStruct((8, 16), f32), til...  35.4 us
    unnamed x8, local copies, waits for them, and re-layouts  1.28 us

profile of v1, /device:TPU:1, one launch (start us, length us, event | category | flops | bytes accessed | tf_op | source)
XLA Modules:
  0.0 39.5 jit_solution(18021698491885291181)
XLA Ops:
  0.6 35.4 %decode_step.1 = (f32[8,16]{1,0:T(8,128)}, f32[8,128]{1,0:T(8,128)}, f32[8,128]{1,0:T(8,128)}, f32[8,128]{1,0:T(8,128)}) custom-call(bf16[8,16]{1,0:T(8,128)(2,1)} %tok_h.1, f32[1,16]{1,0:T(1,128)} %bitcast.19, bf16[16,2,64]{2,1,0:T(2,128)(2,1)} %wq_h.1, bf16[16,2,64]{2,1,0:T(2,128)(2,1)} %wk_h.1, bf16[16,2,64]{2,1,0:T(2,128)(2,1)} %wv_h.1, ...), custom_call_target="tpu_custom_call" | custom-call | tf_op jit(solution)/shard_map/decode_step/pallas_call | solution.py:300
  36.1 0.8 %reshape.33 = f32[8,2,64]{2,1,0:T(2,128)S(1)} reshape(f32[8,128]{1,0:T(8,128)} %get-tuple-element.11) | data formatting | bytes 8192 | tf_op jit(solution)/shard_map/reshape | solution.py:311
  36.8 0.0 copy-start
  36.8 0.6 %copy.17 = f32[8,2,1]{0,1,2:T(2,128)} copy(f32[8,2,1]{2,1,0:T(2,128)S(1)} %bitcast.15) | data formatting | bytes 128
  37.5 0.0 copy-done
  37.5 0.0 copy-start.1
  37.5 0.7 %reshape.32 = f32[8,2,64]{2,1,0:T(2,128)} reshape(f32[8,128]{1,0:T(8,128)S(1)} %copy-done) | data formatting | bytes 8192 | tf_op jit(solution)/shard_map/reshape | solution.py:310
  38.2 0.0 copy-done.1
  38.2 0.0 copy-start.2
  38.2 0.7 %convert_element_type.7 = bf16[8,2,64]{2,1,0:T(2,128)(2,1)} reshape(bf16[8,128]{1,0:T(8,128)(2,1)S(1)} %convert_element_type.6) | data formatting | bytes 4096 | tf_op jit(solution)/shard_map/convert_element_type | solution.py:309
  38.9 0.0 copy-done.2
  38.9 0.6 %copy.19 = f32[8,16]{1,0:T(8,128)} copy(f32[8,16]{1,0:T(8,128)S(1)} %copy-done.2) | data formatting | bytes 1024
  (1 shorter events, 0.0 us)
Async XLA Ops:
  36.8 0.7 %copy-start = (f32[8,128]{1,0:T(8,128)S(1)}, f32[8,128]{1,0:T(8,128)}, u32[]{:S(2)}) copy-start(f32[8,128]{1,0:T(8,128)} %get-tuple-element.10) | copy-start | bytes 12292
  37.5 0.7 %copy-start.1 = (f32[8,128]{1,0:T(8,128)S(1)}, f32[8,128]{1,0:T(8,128)}, u32[]{:S(2)}) copy-start(f32[8,128]{1,0:T(8,128)} %get-tuple-element.9) | copy-start | bytes 12292
  38.2 0.7 %copy-start.2 = (f32[8,16]{1,0:T(8,128)S(1)}, f32[8,16]{1,0:T(8,128)}, u32[]{:S(2)}) copy-start(f32[8,16]{1,0:T(8,128)} %get-tuple-element.16) | copy-start | bytes 1540

commit v2 on v1

--- a/solution.py
+++ b/solution.py
@@ -50,27 +50,26 @@
 def kernel(
     tok_h, gain_h, wq_h, wk_h, wv_h, wg_h, wf_h, wo_h, key_h, val_h, logf_h, len_h,
     mixed_o, nkey_o, nval_o, nlogf_o,
-    tok, gain, wq, wk, wv, wg, wf, wo, key, val, logf, lens, small_sem, logf_sem, key_sem, val_sem,
+    tok, gain, wq, wk, wv, wg, wf, wo, key, val, logf, lens, small_sem, key_sem, val_sem,
     crit, rs_src, rs, ar, ag, tpb, bias_s, side, send_sem, recv_sem,
 ):
     z, y, t = lax.axis_index("kv_0"), lax.axis_index("kv_1"), lax.axis_index("tp")
-    barrier = pltpu.get_barrier_semaphore()
-    for d in FAR_FIRST:
-        pl.semaphore_signal(barrier, 1, device_id={"kv_1": lax.rem(y + d, N)}, device_id_type=MESH)
-        pl.semaphore_signal(barrier, 1, device_id={"kv_0": lax.rem(z + d, N)}, device_id_type=MESH)
-    pl.semaphore_signal(barrier, 1, device_id={"tp": 1 - t}, device_id_type=MESH)
-
     smalls = [
         pltpu.make_async_copy(a, b, small_sem.at[i])
         for i, (a, b) in enumerate(
-            [(tok_h, tok), (gain_h, gain), (wq_h, wq), (wk_h, wk), (wv_h, wv), (wg_h, wg), (wf_h, wf),
-             (len_h, lens), (wo_h, wo)]
+            [(tok_h, tok), (gain_h, gain), (wq_h, wq), (wf_h, wf), (wk_h, wk), (wv_h, wv), (wg_h, wg),
+             (len_h, lens), (logf_h, logf), (wo_h, wo)]
         )
     ]
-    for copy in smalls:
+    for copy in smalls[:4]:
         copy.start()
-    logf_copy = pltpu.make_async_copy(logf_h, logf, logf_sem)
-    logf_copy.start()
+    barrier = pltpu.get_barrier_semaphore()
+    for d in FAR_FIRST:
+        pl.semaphore_signal(barrier, 1, device_id={"kv_1": (y + d) & 7}, device_id_type=MESH)
+        pl.semaphore_signal(barrier, 1, device_id={"kv_0": (z + d) & 7}, device_id_type=MESH)
+    pl.semaphore_signal(barrier, 1, device_id={"tp": 1 - t}, device_id_type=MESH)
+    for copy in smalls[4:]:
+        copy.start()
     key_copies = [
         pltpu.make_async_copy(key_h.at[pl.ds(i * 256, 256)], key.at[pl.ds(i * 256, 256)], key_sem.at[i])
         for i in range(4)
@@ -86,7 +85,7 @@
         for d in FAR_FIRST:
             pltpu.make_async_remote_copy(
                 src, buf.at[me], send_sem.at[stage], recv_sem.at[stage],
-                device_id={axis: lax.rem(me + d, N)}, device_id_type=MESH,
+                device_id={axis: (me + d) & 7}, device_id_type=MESH,
             ).start()
 
     def arrived(stage, buf):
@@ -97,7 +96,7 @@
         seven = buf.at[pl.ds(0, N - 1)]
         pltpu.make_async_copy(seven, seven, send_sem.at[stage]).wait()
 
-    for copy in smalls:
+    for copy in smalls[:4]:
         copy.wait()
     wide = tok[...].astype(jnp.float32)
     squares = lane_sum(wide * wide)
@@ -115,14 +114,19 @@
     wf32 = wf[...].astype(jnp.float32)
     narrow32 = narrow.astype(jnp.float32)
     forget = [lane_sum(narrow32 * wf32[h : h + 1, :]) for h in range(2)]
-
+    crit[0, y, 0:8, :] = project(wq)
+    crit[0, y, 8:9, :] = to_row([squares, forget[0], forget[1]])
+    pl.semaphore_wait(barrier, 15)
+    exchange(0, crit.at[0], crit.at[0, y], "kv_1", y)
+
+    for copy in smalls[4:]:
+        copy.wait()
     sub8, lane8 = iota((8, 8), 0), iota((8, 8), 1)
     len_col = lane_sum(jnp.where(sub8 == lane8, lens[...].astype(jnp.float32), 0.0))
     len_col = jnp.concatenate([len_col, len_col], axis=0)
     first = (z * N + y) * 512
     position = (iota((16, 512), 1) + first).astype(jnp.float32)
     valid = position < len_col
-    logf_copy.wait()
     gates = jnp.concatenate([logf[:, 0, :], logf[:, 1, :]], axis=0)
     gates = jnp.where(valid, gates, 0.0)
     blocks = jnp.concatenate([gates[:, 128 * j : 128 * (j + 1)] for j in range(4)], axis=0)
@@ -133,18 +137,14 @@
     for j in (3, 2, 1, 0):
         bias_s[:, 128 * j : 128 * (j + 1)] = sums[16 * j : 16 * (j + 1), :128] + later
         later = later + sums[16 * j : 16 * (j + 1), 128:]
-
-    crit[0, y, 0:8, :] = project(wq)
-    crit[0, y, 8:9, :] = to_row([squares, forget[0], forget[1], later[:8], later[8:]])
     pieces = [project(wk), project(wv), project(wg)]
+    shard_row = to_row([later[:8], later[8:]])
     for j in range(N):
         for i, piece in enumerate(pieces):
             rs_src[j, :, 128 * i : 128 * (i + 1)] = piece[j : j + 1, :]
-
-    pl.semaphore_wait(barrier, 15)
-    exchange(0, crit.at[0], crit.at[0, y], "kv_1", y)
+        rs_src[j, :, 384:512] = shard_row
     for d in FAR_FIRST:
-        other = lax.rem(y + d, N)
+        other = (y + d) & 7
         pltpu.make_async_remote_copy(
             rs_src.at[other], rs.at[y], send_sem.at[4], recv_sem.at[4],
             device_id={"kv_1": other}, device_id_type=MESH,
@@ -157,10 +157,10 @@
             acc = acc + crit[stage, j]
         return acc
 
-    def later_rows(stage, me):
+    def later_rows(buf, me):
         acc = jnp.zeros((1, 128), jnp.float32)
         for j in range(1, N):
-            acc = acc + jnp.where(j > me, crit[stage, j, 8:9, :], 0.0)
+            acc = acc + jnp.where(j > me, buf[j, :, 384:512], 0.0)
         return acc
 
     arrived(0, crit.at[0])
@@ -174,7 +174,7 @@
     ar[z] = row
     exchange(5, ar, ar.at[z], "kv_0", z)
 
-    later_y = later_rows(0, y)
+    later_y = later_rows(rs, y)
     for copy in key_copies:
         copy.wait()
 
@@ -193,8 +193,6 @@
     for h in range(2):
         logit = from_row(info, 1 + h) * inv_root
         new_logf.append(jnp.minimum(logit, 0.0) - jnp.log1p(jnp.exp(-jnp.abs(logit))))
-    later_all = later_y + later_rows(1, z)
-    extra = jnp.concatenate([from_row(later_all, 3) + new_logf[0], from_row(later_all, 4) + new_logf[1]], axis=0)
 
     q32 = side[0]
     double = jnp.concatenate([q32, q32], axis=0)
@@ -204,7 +202,7 @@
         [jnp.where(own_head & (row16 % 8 == b), double, 0.0).astype(jnp.bfloat16) for b in range(8)], axis=1
     )
     scores = jnp.dot(lhs, key[...], preferred_element_type=jnp.float32) * (HD ** -0.5)
-    weights = jnp.where(valid, jnp.exp(scores + (bias_s[...] + extra)), 0.0)
+    weights = jnp.where(valid, jnp.exp(scores + bias_s[...]), 0.0)
     den = lane_sum(weights)
     for copy in val_copies:
         copy.wait()
@@ -214,11 +212,13 @@
     acc = jnp.zeros((16, 128), jnp.float32)
     for b in range(8):
         acc = jnp.where(own_head & (row16 % 8 == b), wide_out[:, 128 * b : 128 * (b + 1)], acc)
-    crit[2, y, 0:8, :] = acc[:8] + acc[8:]
-    crit[2, y, 8:9, :] = to_row([den[:8], den[8:]])
+    arrived(5, ar)
+    later_all = later_y + later_rows(ar, z)
+    decay = [jnp.exp(from_row(later_all, h) + new_logf[h]) for h in range(2)]
+    crit[2, y, 0:8, :] = (acc[:8] + acc[8:]) * by_head(decay[0], decay[1])
+    crit[2, y, 8:9, :] = to_row([den[:8] * decay[0], den[8:] * decay[1]])
     exchange(2, crit.at[2], crit.at[2, y], "kv_1", y)
 
-    arrived(5, ar)
     row = ar[0]
     for j in range(1, N):
         row = row + ar[j]
@@ -240,9 +240,10 @@
     silu = gate * jax.nn.sigmoid(gate)
     score_new = head_mean(side[0] * key_new32) * (HD ** 0.5)
     weight_new = jnp.exp(score_new)
-    nkey_o[...] = key_new32
-    nval_o[...] = value_new
-    nlogf_o[...] = by_head(new_logf[0], new_logf[1])
+    for h in range(2):
+        nval_o[:, h, :] = value_new[:, HD * h : HD * (h + 1)]
+        nlogf_o[h : h + 1, :] = to_row([new_logf[h]])[:, :8]
+    nkey_o[...] = jnp.stack([key_new32[:, :HD], key_new32[:, HD:]], axis=1).astype(jnp.bfloat16)
 
     arrived(3, crit.at[3])
     summed = total(3)
@@ -270,6 +271,17 @@
     mixed_o[...] = tpb[0] + tpb[1]
 
 
+def write_out(a, b, c, d, a_h, b_h, c_h, d_h, sem):
+    copies = [
+        pltpu.make_async_copy(src, dst, sem.at[i])
+        for i, (src, dst) in enumerate([(a, a_h), (b, b_h), (c, c_h), (d, d_h)])
+    ]
+    for copy in copies:
+        copy.start()
+    for copy in copies:
+        copy.wait()
+
+
 def on_device(tokens, norm_gain, w_query, w_key, w_value, w_gate, w_forget, w_out, cache_key, cache_value, cache_logf, lengths):
     span = cache_key.shape[1]
     keys = jnp.transpose(cache_key, (0, 2, 3, 1)).reshape(8 * 2 * HD, span)
@@ -282,33 +294,39 @@
     f32 = jnp.float32
     tile = jax.ShapeDtypeStruct((8, 128), f32)
     scratch = [pltpu.VMEM(a.shape, a.dtype) for a in args] + [
-        pltpu.SemaphoreType.DMA((9,)),
-        pltpu.SemaphoreType.DMA(()),
+        pltpu.SemaphoreType.DMA((10,)),
         pltpu.SemaphoreType.DMA((4,)),
         pltpu.SemaphoreType.DMA((4,)),
         pltpu.VMEM((4, N, 9, 128), f32),
-        pltpu.VMEM((N, 1, 384), f32),
-        pltpu.VMEM((N, 1, 384), f32),
-        pltpu.VMEM((N, 1, 384), f32),
-        pltpu.VMEM((N, 1, 384), f32),
+        pltpu.VMEM((N, 1, 512), f32),
+        pltpu.VMEM((N, 1, 512), f32),
+        pltpu.VMEM((N, 1, 512), f32),
+        pltpu.VMEM((N, 1, 512), f32),
         pltpu.VMEM((2, 8, 16), f32),
         pltpu.VMEM((16, 512), f32),
         pltpu.VMEM((1, 8, 128), f32),
         pltpu.SemaphoreType.DMA((8,)),
         pltpu.SemaphoreType.DMA((8,)),
     ]
-    mixed, nkey, nval, nlogf = pl.pallas_call(
+    shapes = [((8, 16), f32), ((8, 2, HD), jnp.bfloat16), ((8, 2, HD), f32), ((2, 8), f32)]
+    results = pl.pallas_call(
         kernel,
-        out_shape=(jax.ShapeDtypeStruct((8, 16), f32), tile, tile, tile),
+        out_shape=tuple(pltpu.VMEM(*a) for a in shapes),
         in_specs=[pl.BlockSpec(memory_space=pltpu.HBM)] * 12,
-        out_specs=tuple(pl.BlockSpec(memory_space=pltpu.VMEM) for _ in range(4)),
+        out_specs=tuple(pl.BlockSpec(memory_space=pltpu.VMEM) for _ in shapes),
         scratch_shapes=scratch,
         compiler_params=pltpu.CompilerParams(collective_id=0, has_side_effects=True),
         name="decode_step",
     )(*args)
-    key_new = nkey.reshape(8, 2, HD).astype(jnp.bfloat16)
-    value_new = nval.reshape(8, 2, HD)
-    return mixed, key_new, value_new, nlogf.reshape(8, 2, HD)[:, :, 0]
+    mixed, key_new, value_new, logf_new = pl.pallas_call(
+        write_out,
+        out_shape=tuple(jax.ShapeDtypeStruct(*a) for a in shapes),
+        in_specs=[pl.BlockSpec(memory_space=pltpu.VMEM)] * 4,
+        out_specs=tuple(pl.BlockSpec(memory_space=pltpu.HBM) for _ in shapes),
+        scratch_shapes=[pltpu.SemaphoreType.DMA((4,))],
+        name="write_out",
+    )(*(pltpu.with_memory_space_constraint(r, pltpu.VMEM) for r in results))
+    return mixed, key_new, value_new, logf_new.T
 
 
 def solution(mesh):

time: 39.8 us -> 36.4 us (0.915)
  local copies, waits for them, and re-layouts: 3.39 us -> 0 us
    reshape x2 -> x0, local copies, waits for them, and re-layouts: 1.43 us -> none  [the longest x1 0.76 us: on_device(): return (mixed, key_new, value_new, nlogf.reshape(8, 2, HD)[:, :, 0])]
    unnamed x8 -> x0, local copies, waits for them, and re-layouts: 1.28 us -> none
    convert_element_type x1 -> x0, local copies, waits for them, and re-layouts: 0.67 us -> none  [on_device(): key_new = nkey.reshape(8, 2, HD).astype(jnp.bfloat16)]
    pallas_call x1 -> x2, Pallas kernels: 35.4 us -> 35.6 us  [the longest x1 34.9 us: on_device(): pl.pallas_call(kernel, out_shape=tuple((pltpu.VMEM(*a) for a in shapes)),...]
where the time goes in v2:
time: 36.4 us; the launch traced here: 36.2 us
  Pallas kernels  35.6 us (98%)
  between operations  0.64 us (2%)
    pallas_call x1, Pallas kernels, on_device(): pl.pallas_call(kernel, out_shape=tuple((pltpu.VMEM(*a) for a in shapes)),...  34.9 us

profile of v2, /device:TPU:1, one launch (start us, length us, event | category | flops | bytes accessed | tf_op | source)
XLA Modules:
  0.0 36.2 jit_solution(13317091241537952385)
XLA Ops:
  0.6 34.9 %decode_step.1 = (f32[8,16]{1,0:T(8,128)S(1)}, bf16[8,2,64]{2,1,0:T(2,128)(2,1)S(1)}, f32[8,2,64]{2,1,0:T(2,128)S(1)}, f32[2,8]{1,0:T(2,128)S(1)}) custom-call(bf16[8,16]{1,0:T(8,128)(2,1)} %tok_h.1, f32[1,16]{1,0:T(1,128)} %bitcast.16, bf16[16,2,64]{2,1,0:T(2,128)(2,1)} %wq_h.1, bf16[16,2,64]{2,1,0:T(2,128)(2,1)} %wk_h.1, bf16[16,2,64]{2,1,0:T(2,128)(2,1)} %wv_h.1, ...), custom_call_target="tpu_custom_call" | custom-call | tf_op jit(solution)/shard_map/decode_step/pallas_call | solution.py:312
  35.6 0.6 %write_out.1 = (f32[8,16]{1,0:T(8,128)}, bf16[8,2,64]{2,1,0:T(2,128)(2,1)}, f32[8,2,64]{2,1,0:T(2,128)}, f32[2,8]{1,0:T(2,128)}) custom-call(f32[8,16]{1,0:T(8,128)S(1)} %get-tuple-element.12.a, bf16[8,2,64]{2,1,0:T(2,128)(2,1)S(1)} %get-tuple-element.13.b, f32[8,2,64]{2,1,0:T(2,128)S(1)} %get-tuple-element.14.c, f32[2,8]{1,0:T(2,128)S(1)} %get-tuple-element.15.d), custom_call_target="tpu_custom_call" | custom-call | tf_op jit(solution)/shard_map/write_out/pallas_call | solution.py:321
